TPU v7x, 32 devices: a whole 2x2x4 slice. The times are simulated.
32 devices in a mesh: fs: 8 (over z, y), tp: 4 (over x, core).
Axes of the slice: x: 2, y: 2, z: 4, core: 2. Of those that a mesh axis runs over, the one named last changes fastest.
Arguments:
- tokens: bfloat16 [8192, 2048], P('fs'), may hold values from -6 to 6
- norm_gain: float32 [2048], P('fs'), may hold values from 0.1 to 1.9
- gate_train: float32 [8, 2048, 768], P(None, 'fs', 'tp'), may hold values from -0.125 to 0.125
- up_train: float32 [8, 2048, 768], P(None, 'fs', 'tp'), may hold values from -0.125 to 0.125
- down_train: float32 [8, 768, 2048], P(None, 'fs', 'tp'), may hold values from -0.21875 to 0.21875
- expert_ids: int32 [8192, 2], P('fs'), may hold values from 0 to 7, all different within a row; in each aligned block of 1024 rows (0 to 1023, 1024 to 2047, ...) at most 512 rows name the same one
- route_weights: float32 [8192, 2], P('fs'), may hold values from 0.1 to 1
Outputs:
- gate_serve: bfloat16 [8, 2048, 768], P('fs', None, 'tp')
- up_serve: bfloat16 [8, 2048, 768], P('fs', None, 'tp')
- down_serve: bfloat16 [8, 768, 2048], P('fs', 'tp')
- mixed: bfloat16 [8192, 2048], P('fs', 'tp')
Inputs may be any that keep to these rules, and one draw needn't show every extreme that they name: `expert_ids`: each row names 2 different experts. Within each aligned block of 1024 rows no expert is named more than 512 times, and in every block some expert is named exactly 512 times; every expert is named somewhere.
All inputs are finite; a program needn't handle non-finite values.
Results may differ from a plain program's by a relative error of at most 0.011.
Values may be sent and summed in bfloat16 or wider, within the bound.
A program may use at most 128 MiB of HBM per device.

v0:
```python
import jax
import jax.numpy as jnp
from jax import lax
from jax.sharding import PartitionSpec as P

epsilon = 1e-06


def on_device(tokens, norm_gain, gate_train, up_train, down_train, expert_ids, route_weights):
    fs_count = lax.axis_size("fs")
    tp_count = lax.axis_size("tp")
    experts = gate_train.shape[0]
    local_experts = experts // fs_count
    gate_cast = (norm_gain[None, :, None] * gate_train).astype(jnp.bfloat16)
    up_cast = (norm_gain[None, :, None] * up_train).astype(jnp.bfloat16)
    gate_serve, up_serve = (
        lax.all_to_all(gate_cast, "fs", split_axis=0, concat_axis=1, tiled=True),
        lax.all_to_all(up_cast, "fs", split_axis=0, concat_axis=1, tiled=True),
    )
    down_serve = lax.all_to_all(
        lax.all_to_all(
            down_train.astype(jnp.bfloat16), "fs", split_axis=0, concat_axis=1, tiled=True
        ),
        "tp",
        split_axis=1,
        concat_axis=2,
        tiled=True,
    )
    tok_float = tokens.astype(jnp.float32)
    normed = (
        tok_float * lax.rsqrt(jnp.mean(tok_float * tok_float, axis=-1, keepdims=True) + epsilon)
    ).astype(jnp.bfloat16)
    tok_rows, picks = expert_ids.shape
    width = tokens.shape[1]
    capacity = 2 * tok_rows * picks // experts
    flat_ids = expert_ids.reshape(-1)
    onehot = (flat_ids[:, None] == jnp.arange(experts, dtype=jnp.int32)[None, :]).astype(jnp.int32)
    slot_rank = jnp.sum((jnp.cumsum(onehot, axis=0) - onehot) * onehot, axis=1)
    target = (flat_ids * capacity + slot_rank).reshape(tok_rows, picks)
    slot_ids = jnp.arange(experts * capacity, dtype=jnp.int32)
    dispatch = jnp.zeros((experts * capacity, tok_rows), jnp.bfloat16)
    for pick in range(picks):
        dispatch = dispatch + (slot_ids[:, None] == target[None, :, pick]).astype(jnp.bfloat16)
    outgoing = jnp.dot(dispatch, normed, preferred_element_type=jnp.float32).astype(jnp.bfloat16)
    outgoing = outgoing.reshape(experts, capacity, width)
    quarter = capacity // tp_count
    gate_whole, up_whole, down_whole = (
        lax.all_gather(gate_serve, "tp", axis=2, tiled=True),
        lax.all_gather(up_serve, "tp", axis=2, tiled=True),
        lax.all_gather(down_serve, "tp", axis=1, tiled=True),
    )
    share_rows = lax.dynamic_slice_in_dim(outgoing, lax.axis_index("tp") * quarter, quarter, 1)
    routed = lax.all_to_all(share_rows, "fs", split_axis=0, concat_axis=1, tiled=True)
    gate_act = jnp.einsum("erd,edf->erf", routed, gate_whole, preferred_element_type=jnp.float32)
    up_act = jnp.einsum("erd,edf->erf", routed, up_whole, preferred_element_type=jnp.float32)
    hidden = (jax.nn.silu(gate_act) * up_act).astype(jnp.bfloat16)
    row_count = hidden.shape[1]
    block_width = hidden.shape[2] // tp_count
    hidden_blocks = hidden.reshape(local_experts, row_count, tp_count, block_width)
    down_blocks = down_whole.reshape(local_experts, tp_count, block_width, width)
    partial_value = jnp.einsum(
        "erbf,ebfd->erbd", hidden_blocks, down_blocks, preferred_element_type=jnp.float32
    )
    results = jnp.sum(partial_value.astype(jnp.bfloat16).astype(jnp.float32), axis=2).astype(
        jnp.bfloat16
    )
    returned = lax.all_to_all(
        lax.all_to_all(results, "fs", split_axis=1, concat_axis=0, tiled=True),
        "tp",
        split_axis=2,
        concat_axis=1,
        tiled=True,
    )
    returned_flat = returned.reshape(experts * capacity, returned.shape[2])
    shares = route_weights / jnp.sum(route_weights, axis=-1, keepdims=True)
    mixed = jnp.zeros((tok_rows, returned_flat.shape[1]), jnp.float32)
    for pick in range(picks):
        selector = (target[:, pick][:, None] == slot_ids[None, :]).astype(jnp.bfloat16)
        picked = jnp.dot(selector, returned_flat, preferred_element_type=jnp.float32)
        mixed = mixed + shares[:, pick][:, None] * picked
    return (gate_serve, up_serve, down_serve, mixed.astype(jnp.bfloat16))


def solution(mesh):
    return jax.shard_map(
        on_device,
        mesh=mesh,
        in_specs=(
            P("fs", None),
            P("fs"),
            P(None, "fs", "tp"),
            P(None, "fs", "tp"),
            P(None, "fs", "tp"),
            P("fs", None),
            P("fs", None),
        ),
        out_specs=(P("fs", None, "tp"), P("fs", None, "tp"), P("fs", "tp", None), P("fs", "tp")),
        check_vma=False,
    )
```

profile of v0, /device:TPU:0, one launch (start us, length us, event | category | flops | bytes accessed | tf_op | source)
XLA Modules:
  0.0 500.3 jit_solution(15567781841299172667)
XLA Ops:
  10.7 7.3 %all-to-all-start.1 = ((bf16[8,256,192]{1,2,0:T(8,128)(2,1)}), bf16[8,256,192]{1,2,0:T(8,128)(2,1)S(1)}, u32[]{:S(2)}, u32[]{:S(2)}) async-start(bf16[8,256,192]{1,2,0:T(8,128)(2,1)} %get-tuple-element.8), calls=%async_computation.1 | async-start | bytes 1572864 | tf_op jit(solution)/shard_map/all_to_all | solution.py:18
  19.0 19.2 %all-to-all-done.1 = bf16[8,256,192]{1,2,0:T(8,128)(2,1)S(1)} async-done(((bf16[8,256,192]{1,2,0:T(8,128)(2,1)}), bf16[8,256,192]{1,2,0:T(8,128)(2,1)S(1)}, u32[]{:S(2)}, u32[]{:S(2)}) %all-to-all-start.1) | async-done | bytes 786464 | tf_op jit(solution)/shard_map/all_to_all | solution.py:18
  45.2 16.9 %all-to-all-done.2 = bf16[8,96,512]{2,1,0:T(8,128)(2,1)S(1)} async-done(((bf16[8,96,512]{2,1,0:T(8,128)(2,1)}), bf16[8,96,512]{2,1,0:T(8,128)(2,1)S(1)}, u32[]{:S(2)}, u32[]{:S(2)}) %all-to-all-start.2) | async-done | bytes 786464 | tf_op jit(solution)/shard_map/all_to_all | solution.py:21
  74.2 5.4 %reduce.7 = bf16[768,512]{1,0:T(8,128)(2,1)S(1)} reduce(bf16[768,1,512]{2,1,0:T(2,128)(2,1)S(1)} %bitcast.68, bf16[]{:T(256)} %broadcast.37), dimensions={1}, to_apply=%bitcast.63.reduce_sub_computation | reduce | bytes 1572866
  81.0 5.0 %all-to-all-done = bf16[8,256,192]{1,2,0:T(8,128)(2,1)S(1)} async-done(((bf16[8,256,192]{1,2,0:T(8,128)(2,1)}), bf16[8,256,192]{1,2,0:T(8,128)(2,1)S(1)}, u32[]{:S(2)}, u32[]{:S(2)}) %all-to-all-start) | async-done | bytes 786464 | tf_op jit(solution)/shard_map/all_to_all | solution.py:17
  89.5 11.2 %all-gather.4.cloned.1.call-start = ((), (), s32[]{:S(2)}) async-start(), calls=%async_computation.7 | async-start | bytes 3932160 | tf_op jit(solution)/shard_map/all_gather | solution.py:48
  100.8 23.5 %convolution_convert_fusion = bf16[4096,2048]{1,0:T(8,128)(2,1)} fusion(s32[1024]{0:T(1024)S(1)} %bitcast.79, s32[1024]{0:T(1024)S(1)} %bitcast.81, bf16[1024,2048]{1,0:T(8,128)(2,1)} %param.7, f32[1024]{0:T(1024)S(1)} %add_rsqrt_fusion), kind=kOutput, calls=%fused_computation.9 | convolution fusion | flops 17228103680 | bytes 20983808 | tf_op jit(solution)/shard_map/dot_general | solution.py:44
  126.0 4.7 constant_dynamic-slice_fusion
  137.4 91.7 %all-to-all-done.4 = bf16[8,128,2048]{2,1,0:T(8,128)(2,1)} async-done(((bf16[8,128,2048]{2,1,0:T(8,128)(2,1)}), bf16[8,128,2048]{2,1,0:T(8,128)(2,1)}, u32[]{:S(2)}, u32[]{:S(2)}) %all-to-all-start.4) | async-done | bytes 4194336 | tf_op jit(solution)/shard_map/all_to_all | solution.py:53
  229.1 8.3 %fusion.15 = f32[1024,768]{0,1:T(8,128)} fusion(bf16[1024,2048]{1,0:T(8,128)(2,1)} %bitcast.7, bf16[1,2048,768]{1,2,0:T(8,128)(2,1)} %all-gather.6.cloned.1.call-done), kind=kOutput, calls=%fused_computation.20 | convolution fusion | flops 3221225472 | bytes 10485760 | tf_op jit(solution)/shard_map/erd,edf->erf/dot_general | solution.py:55
  237.5 7.9 %multiply_convert_fusion = bf16[1024,768]{0,1:T(8,128)(2,1)S(1)} fusion(f32[1024,768]{0,1:T(8,128)} %fusion.15, bf16[1024,2048]{1,0:T(8,128)(2,1)} %bitcast.7, bf16[1,2048,768]{1,2,0:T(8,128)(2,1)} %all-gather.4.cloned.1.call-done), kind=kOutput, calls=%fused_computation.24 | convolution fusion | flops 3225944064 | bytes 12058624 | tf_op jit(solution)/shard_map/erd,edf->erf/dot_general | solution.py:54
  245.4 9.6 %convert_reduce_fusion = bf16[1024,2048]{1,0:T(8,128)(2,1)} fusion(bf16[1024,4,192]{0,2,1:T(8,128)(2,1)S(1)} %bitcast.86, bf16[4,192,2048]{2,1,0:T(8,128)(2,1)} %bitcast.85), kind=kOutput, calls=%fused_computation.1 | convolution fusion | flops 3235905536 | bytes 8912896 | tf_op jit(solution)/shard_map/erbf,ebfd->erbd/dot_general | solution.py:61
  255.0 8.6 %copy.77 = bf16[1,1024,2048]{2,0,1:T(2,128)(2,1)} copy(bf16[1,1024,2048]{2,1,0:T(8,128)(2,1)} %bitcast.70) | data formatting | bytes 8388608 | tf_op jit(solution)/shard_map/reduce_sum | solution.py:64
  263.6 26.9 %reduce.8 = bf16[1024,2048]{1,0:T(8,128)(2,1)} reduce(bf16[1024,1,2048]{2,1,0:T(2,128)(2,1)} %bitcast.65, bf16[]{:T(256)} %broadcast.37), dimensions={1}, to_apply=%bitcast.62.reduce_sub_computation | reduce | bytes 8388610
  290.5 7.8 %reshape.108 = bf16[8,2,131072]{2,1,0:T(2,128)(2,1)} reshape(bf16[1024,2048]{1,0:T(8,128)(2,1)} %reduce.8) | data formatting | bytes 8388608
  298.3 97.7 %all_to_all.90 = bf16[8,2,131072]{2,1,0:T(2,128)(2,1)} all-to-all(bf16[8,2,131072]{2,1,0:T(2,128)(2,1)} %reshape.108), channel_id=1, replica_groups=mesh['fs'=8,'tp'=4] {'fs'}, dimensions={0} | all-to-all | bytes 8388608 | tf_op jit(solution)/shard_map/all_to_all | solution.py:68
  396.0 8.7 %reshape.109 = bf16[1024,1,2048]{2,1,0:T(2,128)(2,1)} reshape(bf16[8,2,131072]{2,1,0:T(2,128)(2,1)} %all_to_all.90) | data formatting | bytes 8388608
  404.7 8.0 %copy.71 = bf16[1,1024,2048]{2,1,0:T(8,128)(2,1)} copy(bf16[1,1024,2048]{2,0,1:T(2,128)(2,1)} %bitcast.66) | data formatting | bytes 8388608
  412.7 6.8 %copy.66 = bf16[8,128,2048]{1,0,2:T(8,128)(2,1)} copy(bf16[8,128,2048]{2,1,0:T(8,128)(2,1)} %bitcast.67) | data formatting | bytes 8388608 | tf_op jit(solution)/shard_map/all_to_all | solution.py:68
  419.5 5.0 all-to-all-start.6
  424.6 48.1 %all-to-all-done.6 = bf16[8,128,2048]{1,0,2:T(8,128)(2,1)} async-done(((bf16[8,128,2048]{1,0,2:T(8,128)(2,1)}), bf16[8,128,2048]{1,0,2:T(8,128)(2,1)}, u32[]{:S(2)}, u32[]{:S(2)}) %all-to-all-start.6) | async-done | bytes 4194336 | tf_op jit(solution)/shard_map/all_to_all | solution.py:67
  472.7 7.6 %copy.68 = bf16[8,4,128,512]{3,2,1,0:T(8,128)(2,1)} copy(bf16[8,4,128,512]{2,0,3,1:T(8,128)(2,1)} %bitcast.15) | data formatting | bytes 8388608 | tf_op jit(solution)/shard_map/all_to_all | solution.py:67
  480.3 7.5 %fusion = f32[1024,512]{1,0:T(8,128)S(1)} fusion(bf16[4096,512]{1,0:T(8,128)(2,1)} %bitcast.71, s32[1024]{0:T(1024)S(1)} %bitcast.82), kind=kOutput, calls=%fused_computation.5 | convolution fusion | flops 4299161600 | bytes 6295552 | tf_op jit(solution)/shard_map/dot_general | solution.py:79
  487.8 5.6 %add_convert_fusion = bf16[1024,512]{1,0:T(8,128)(2,1)} fusion(f32[1024,512]{1,0:T(8,128)S(1)} %fusion, bf16[4096,512]{1,0:T(8,128)(2,1)S(1)} %bitcast.72, s32[1024]{0:T(1024)S(1)} %bitcast.80, f32[1024]{0:T(1024)S(1)} %bitcast.84, f32[1024]{0:T(1024)S(1)} %bitcast.83), kind=kOutput, calls=%fused_computation.25 | convolution fusion | flops 4301258752 | bytes 7352320 | tf_op jit(solution)/shard_map/dot_general | solution.py:79
  (53 shorter events, 36.8 us)
Async XLA Ops:
  7.2 10.8 %copy-start.2 = (f32[8,96,512]{2,1,0:T(8,128)S(1)}, f32[8,96,512]{2,1,0:T(8,128)}, u32[]{:S(2)}) copy-start(f32[8,96,512]{2,1,0:T(8,128)} %param.11) | copy-start | bytes 4718596
  7.2 34.5 %copy-start.3 = (s32[1024,2]{0,1:T(2,128)S(1)}, s32[1024,2]{0,1:T(2,128)}, u32[]{:S(2)}) copy-start(s32[1024,2]{0,1:T(2,128)} %param.12) | copy-start | bytes 24580
  10.7 27.5 %all-to-all-start.1 = ((bf16[8,256,192]{1,2,0:T(8,128)(2,1)}), bf16[8,256,192]{1,2,0:T(8,128)(2,1)S(1)}, u32[]{:S(2)}, u32[]{:S(2)}) async-start(bf16[8,256,192]{1,2,0:T(8,128)(2,1)} %get-tuple-element.8), calls=%async_computation.1 | async-start | bytes 1572864 | tf_op jit(solution)/shard_map/all_to_all | solution.py:18
  38.1 24.0 %all-to-all-start.2 = ((bf16[8,96,512]{2,1,0:T(8,128)(2,1)}), bf16[8,96,512]{2,1,0:T(8,128)(2,1)S(1)}, u32[]{:S(2)}, u32[]{:S(2)}) async-start(bf16[8,96,512]{2,1,0:T(8,128)(2,1)} %convert_element_type.50), calls=%async_computation.2 | async-start | bytes 1572864 | tf_op jit(solution)/shard_map/all_to_all | solution.py:21
  62.1 3.7 copy-start.1
  62.1 23.9 %all-to-all-start = ((bf16[8,256,192]{1,2,0:T(8,128)(2,1)}), bf16[8,256,192]{1,2,0:T(8,128)(2,1)S(1)}, u32[]{:S(2)}, u32[]{:S(2)}) async-start(bf16[8,256,192]{1,2,0:T(8,128)(2,1)} %get-tuple-element.9), calls=%async_computation | async-start | bytes 1572864 | tf_op jit(solution)/shard_map/all_to_all | solution.py:17
  65.7 71.7 %all-gather.6.cloned.1.call-start = ((), (), s32[]{:S(2)}) async-start(), calls=%async_computation.8 | async-start | bytes 3932160 | tf_op jit(solution)/shard_map/all_gather | solution.py:49
  86.0 44.7 %all-to-all-start.3 = ((bf16[4,2,49152]{2,1,0:T(2,128)(2,1)}), bf16[4,2,49152]{2,1,0:T(2,128)(2,1)S(1)}, u32[]{:S(2)}, u32[]{:S(2)}) async-start(bf16[4,2,49152]{2,1,0:T(2,128)(2,1)} %reshape.106), calls=%async_computation.3 | async-start | bytes 1572864 | tf_op jit(solution)/shard_map/all_to_all | solution.py:20
  89.5 147.9 %all-gather.4.cloned.1.call-start = ((), (), s32[]{:S(2)}) async-start(), calls=%async_computation.7 | async-start | bytes 3932160 | tf_op jit(solution)/shard_map/all_gather | solution.py:48
  130.7 98.4 %all-to-all-start.4 = ((bf16[8,128,2048]{2,1,0:T(8,128)(2,1)}), bf16[8,128,2048]{2,1,0:T(8,128)(2,1)}, u32[]{:S(2)}, u32[]{:S(2)}) async-start(bf16[8,128,2048]{2,1,0:T(8,128)(2,1)} %constant_dynamic-slice_fusion), calls=%async_computation.4 | async-start | bytes 8388608 | tf_op jit(solution)/shard_map/all_to_all | solution.py:53
  135.3 110.0 %all-gather.8.cloned.1.call-start = ((), (), s32[]{:S(2)}) async-start(), calls=%async_computation.9 | async-start | bytes 3932160 | tf_op jit(solution)/shard_map/all_gather | solution.py:50
  419.5 5.0 copy-start.4
  419.5 53.2 %all-to-all-start.6 = ((bf16[8,128,2048]{1,0,2:T(8,128)(2,1)}), bf16[8,128,2048]{1,0,2:T(8,128)(2,1)}, u32[]{:S(2)}, u32[]{:S(2)}) async-start(bf16[8,128,2048]{1,0,2:T(8,128)(2,1)} %copy.66), calls=%async_computation.6 | async-start | bytes 8388608 | tf_op jit(solution)/shard_map/all_to_all | solution.py:67
  480.3 7.5 %copy-start = (bf16[8,4,128,512]{3,2,1,0:T(8,128)(2,1)S(1)}, bf16[8,4,128,512]{3,2,1,0:T(8,128)(2,1)}, u32[]{:S(2)}) copy-start(bf16[8,4,128,512]{3,2,1,0:T(8,128)(2,1)} %copy.68) | copy-start | bytes 12582916
Sparse Core Ops, SparseCore 0:
  70.7 36.2 all-gather.5
  126.1 27.6 all-gather.3
  156.0 28.4 all-gather.7
where the time goes:
time: 509 us; the launch traced here: 500 us
  waiting for transfers between devices  181 us (36%)
  blocking collectives  97.7 us (19%)
  local copies, waits for them, and re-layouts  63.5 us (12%)
  matrix products  62.4 us (12%)
  other arithmetic  42.5 us (8%)
  starting transfers between devices  38.8 us (8%)
  between operations  14.4 us (3%)
    all_to_all x1, blocking collectives, on_device(): lax.all_to_all(results, 'fs', split_axis=1, concat_axis=0, tiled=True)  97.7 us
    all_to_all x1, waiting for transfers between devices, on_device(): lax.all_to_all(share_rows, 'fs', split_axis=0, concat_axis=1, tiled=True)  91.7 us
    all_to_all x1, waiting for transfers between devices, on_device(): lax.all_to_all(lax.all_to_all(results, 'fs', split_axis=1, concat_axis=0,...  48.1 us
    unnamed x3, other arithmetic  32.4 us
    unnamed x18, local copies, waits for them, and re-layouts  27.6 us
    dot_general x1, matrix products, on_device(): jnp.dot(dispatch, normed, preferred_element_type=jnp.float32)  23.5 us
    all_to_all x1, waiting for transfers between devices, on_device(): lax.all_to_all(up_cast, 'fs', split_axis=0, concat_axis=1, tiled=True)  19.2 us
    all_to_all x1, waiting for transfers between devices, on_device(): lax.all_to_all(down_train.astype(jnp.bfloat16), 'fs', split_axis=0, conca...  16.9 us
  transfers between devices with their start and end apart: 9, of which 5 were waited for; matrix products, arithmetic and copies ran while one was open for 13% of the time, Pallas kernels for 0%

commit v1 on v0

v1 whole, which is shorter than its diff:
```python
import jax
import jax.numpy as jnp
from jax import lax
from jax.sharding import PartitionSpec as P

epsilon = 1e-06


def on_device(tokens, norm_gain, gate_train, up_train, down_train, expert_ids, route_weights):
    experts, rows, cols = gate_train.shape
    fs_at = lax.axis_index("fs")
    tok_rows, picks = expert_ids.shape
    down_rows, down_cols = down_train.shape[1:]
    fs_count = lax.axis_size("fs")

    gate_up = jnp.concatenate(
        [norm_gain[None, :, None] * gate_train, norm_gain[None, :, None] * up_train], axis=2
    ).astype(jnp.bfloat16)
    gate_up = gate_up.transpose(1, 0, 2).reshape(rows, experts * 2 * cols)
    gate_up_all = lax.all_gather(gate_up, "fs", axis=0, tiled=True)
    down_all = lax.all_gather(
        down_train.astype(jnp.bfloat16).reshape(experts * down_rows, down_cols),
        "fs", axis=0, tiled=True,
    )

    tok_float = tokens.astype(jnp.float32)
    normed = (
        tok_float * lax.rsqrt(jnp.mean(tok_float * tok_float, axis=-1, keepdims=True) + epsilon)
    ).astype(jnp.bfloat16)
    shares = route_weights / jnp.sum(route_weights, axis=-1, keepdims=True)

    group = 2 * lax.axis_size("tp")
    picked = [jnp.zeros((tok_rows, cols), jnp.float32) for _ in range(picks)]
    for first in range(0, experts, group):
        part = gate_up_all[:, first * 2 * cols : (first + group) * 2 * cols]
        if first:
            part, picked = lax.optimization_barrier((part, picked))
        acts = jnp.dot(normed, part, preferred_element_type=jnp.float32)
        for at in range(group):
            g = acts[:, at * 2 * cols : at * 2 * cols + cols]
            u = acts[:, at * 2 * cols + cols : (at + 1) * 2 * cols]
            h = jax.nn.silu(g) * u
            for k in range(picks):
                picked[k] = picked[k] + jnp.where(
                    expert_ids[:, k : k + 1] == first + at, h, 0.0
                )
    hidden = jnp.stack([picked[k] * shares[:, k : k + 1] for k in range(picks)], 0)
    hidden_all = lax.all_gather(hidden.astype(jnp.bfloat16), "tp", axis=2, tiled=True)
    hidden_all = hidden_all.reshape(picks, tok_rows, fs_count, 1, down_rows)
    ids = jnp.arange(experts, dtype=jnp.int32)[None, None, :, None]
    mixed = jnp.zeros((tok_rows, down_cols), jnp.float32)
    for first in range(0, fs_count, group):
        blocks = hidden_all[:, :, first : first + group]
        if first:
            blocks, mixed = lax.optimization_barrier((blocks, mixed))
        spread = jnp.zeros((tok_rows, group, experts, down_rows), jnp.bfloat16)
        for k in range(picks):
            spread = jnp.where(expert_ids[:, k][:, None, None, None] == ids, blocks[k], spread)
        depth = experts * down_rows
        mixed = mixed + jnp.dot(
            spread.reshape(tok_rows, group * depth),
            down_all[first * depth : (first + group) * depth],
            preferred_element_type=jnp.float32,
        )
    mixed = mixed.astype(jnp.bfloat16)

    own = lax.dynamic_slice_in_dim(gate_up_all, fs_at * 2 * cols, 2 * cols, 1)
    down_own = lax.dynamic_slice_in_dim(
        down_all.reshape(fs_count, experts, down_rows, down_cols), fs_at, 1, 1
    ).reshape(1, fs_count * down_rows, down_cols)
    down_serve = lax.all_to_all(down_own, "tp", split_axis=1, concat_axis=2, tiled=True)
    return own[None, :, :cols], own[None, :, cols:], down_serve, mixed


def solution(mesh):
    return jax.shard_map(
        on_device,
        mesh=mesh,
        in_specs=(
            P("fs", None),
            P("fs"),
            P(None, "fs", "tp"),
            P(None, "fs", "tp"),
            P(None, "fs", "tp"),
            P("fs", None),
            P("fs", None),
        ),
        out_specs=(P("fs", None, "tp"), P("fs", None, "tp"), P("fs", "tp", None), P("fs", "tp")),
        check_vma=False,
    )
```

time: 509 us -> 354 us (0.70); the launches traced: 500 us -> 353 us
  blocking collectives: 97.7 us -> 0 us
  waiting for transfers between devices: 181 us -> 266 us
  local copies, waits for them, and re-layouts: 63.5 us -> 20.5 us
  matrix products: 62.4 us -> 24.7 us
  starting transfers between devices: 38.8 us -> 3.8 us
  other arithmetic: 42.5 us -> 24.4 us
    all_gather x3, waiting for transfers between devices: 0.04 us -> 246 us  [the longest x1 175 us: on_device(): gate_up_all = lax.all_gather(gate_up, 'fs', axis=0, tiled=True)]
    all_to_all x6 -> x1, waiting for transfers between devices: 181 us -> 20.2 us  [on_device(): lax.all_to_all(down_own, 'tp', split_axis=1, concat_axis=2, tiled=True)]
    all_to_all x1 -> x0, blocking collectives: 97.7 us -> none  [on_device(): lax.all_to_all(results, 'fs', split_axis=1, concat_axis=0, tiled=True)]
    dot_general x6 -> x2, matrix products: 62.4 us -> 24.7 us  [the longest x1 17.1 us: on_device(): acts = jnp.dot(normed, part, preferred_element_type=jnp.float32)]
    unnamed x3 -> x2, other arithmetic: 32.4 us -> 5.43 us
    all_to_all x6 -> x1, starting transfers between devices: 27.5 us -> 3.67 us  [on_device(): lax.all_to_all(down_own, 'tp', split_axis=1, concat_axis=2, tiled=True)]
    unnamed x18 -> x16, local copies, waits for them, and re-layouts: 27.6 us -> 4.54 us
    all_to_all x8 -> x1, local copies, waits for them, and re-layouts: 21.1 us -> 0.98 us  [on_device(): lax.all_to_all(down_own, 'tp', split_axis=1, concat_axis=2, tiled=True)]
  transfers between devices with their start and end apart: 9 -> 4, of which waited for: 5 -> 3; matrix products, arithmetic and copies ran while one was open for 13% -> 13% of each run, Pallas kernels for 0% -> 0%
where the time goes in v1:
time: 354 us; the launch traced here: 353 us
  waiting for transfers between devices  266 us (75%)
  matrix products  24.7 us (7%)
  other arithmetic  24.4 us (7%)
  local copies, waits for them, and re-layouts  20.5 us (6%)
  between operations  14 us (4%)
  starting transfers between devices  3.8 us (1%)
    all_gather x1, waiting for transfers between devices, on_device(): gate_up_all = lax.all_gather(gate_up, 'fs', axis=0, tiled=True)  175 us
    all_gather x1, waiting for transfers between devices, on_device(): lax.all_gather(down_train.astype(jnp.bfloat16).reshape(experts * down_row...  71.3 us
    all_to_all x1, waiting for transfers between devices, on_device(): lax.all_to_all(down_own, 'tp', split_axis=1, concat_axis=2, tiled=True)  20.2 us
    dot_general x1, matrix products, on_device(): acts = jnp.dot(normed, part, preferred_element_type=jnp.float32)  17.1 us
    another operation x3, other arithmetic, on_device(): jnp.stack([picked[k] * shares[:, k:k + 1] for k in range(picks)], 0)  9.18 us
    slice x1, local copies, waits for them, and re-layouts, on_device(): blocks[k]  7.82 us
    dot_general x1, matrix products, on_device(): jnp.dot(spread.reshape(tok_rows, group * depth), down_all[first * depth:(...  7.64 us
  transfers between devices with their start and end apart: 4, of which 3 were waited for; matrix products, arithmetic and copies ran while one was open for 13% of the time, Pallas kernels for 0%

profile of v1, /device:TPU:0, one launch (start us, length us, event | category | flops | bytes accessed | tf_op | source)
XLA Modules:
  0.0 353.5 jit_solution(751838854216082823)
XLA Ops:
  7.2 2.3 multiply_convert_fusion.1
  9.6 1.3 pad_maximum_fusion
  10.9 1.0 convert_element_type.14
  12.2 3.1 fusion
  15.4 174.5 %all-gather.4.cloned.1.call-done = bf16[2048,3072]{0,1:T(8,128)(2,1)} async-done(((bf16[256,3072]{0,1:T(8,128)(2,1)}), bf16[2048,3072]{0,1:T(8,128)(2,1)}) %all-gather.4.cloned.1.call-update) | async-done | bytes 12582928 | tf_op jit(solution)/shard_map/all_gather | solution.py:20
  189.9 17.1 %fusion.2 = f32[1024,3072]{1,0:T(8,128)S(1)} fusion(bf16[2048,3072]{0,1:T(8,128)(2,1)} %all-gather.4.cloned.1.call-done, bf16[1024,2048]{1,0:T(8,128)(2,1)} %param.7, f32[1024]{0:T(1024)S(1)} %add_rsqrt_fusion), kind=kOutput, calls=%fused_computation.5 | convolution fusion | flops 12891193344 | bytes 29364224 | tf_op jit(solution)/shard_map/dot_general | solution.py:38
  207.0 4.5 %fusion.5 = bf16[1,1024,192]{2,1,0:T(8,128)(2,1)S(1)} fusion(f32[1024]{0:T(1024)S(1)} %bitcast.47, pred[1024]{0:T(1024)(128)(4,1)S(1)} %get-tuple-element.19, pred[1024]{0:T(1024)(128)(4,1)S(1)} %get-tuple-element.18, pred[1024]{0:T(1024)(128)(4,1)S(1)} %get-tuple-element.17, pred[1024]{0:T(1024)(128)(4,1)S(1)} %get-tuple-element.16, ...), kind=kLoop, calls=%fused_computation.24 | loop fusion | flops 11206656 | bytes 12988416 | tf_op jit(solution)/shard_map/stack | solution.py:47
  211.5 4.5 %fusion.6 = bf16[1,1024,192]{2,1,0:T(8,128)(2,1)S(1)} fusion(f32[1024]{0:T(1024)S(1)} %bitcast.46, pred[1024]{0:T(1024)(128)(4,1)S(1)} %get-tuple-element.12, pred[1024]{0:T(1024)(128)(4,1)S(1)} %get-tuple-element.11, pred[1024]{0:T(1024)(128)(4,1)S(1)} %get-tuple-element.10, pred[1024]{0:T(1024)(128)(4,1)S(1)} %get-tuple-element.9, ...), kind=kLoop, calls=%fused_computation.25 | loop fusion | flops 11206656 | bytes 12988416 | tf_op jit(solution)/shard_map/stack | solution.py:47
  216.2 2.0 copy.22
  218.2 71.3 %all-gather.6.cloned.1.call-done = bf16[6144,512]{1,0:T(8,128)(2,1)} async-done(((bf16[768,512]{1,0:T(8,128)(2,1)}), bf16[6144,512]{1,0:T(8,128)(2,1)}) %all-gather.6.cloned.1.call-update) | async-done | bytes 6291472 | tf_op jit(solution)/shard_map/all_gather | solution.py:21
  289.5 1.2 constant_dynamic-slice_fusion
  290.8 1.2 copy.30
  292.5 5.4 %reduce.32 = bf16[768,512]{1,0:T(8,128)(2,1)S(1)} reduce(bf16[768,1,512]{2,1,0:T(2,128)(2,1)S(1)} %bitcast.37, bf16[]{:T(256)} %broadcast.126), dimensions={1}, to_apply=%bitcast.32.reduce_sub_computation | reduce | bytes 1572866
  297.9 1.4 reshape.117
  299.3 3.7 %all-to-all-start = ((bf16[4,2,49152]{2,1,0:T(2,128)(2,1)}), bf16[4,2,49152]{2,1,0:T(2,128)(2,1)S(1)}, u32[]{:S(2)}, u32[]{:S(2)}) async-start(bf16[4,2,49152]{2,1,0:T(2,128)(2,1)} %reshape.117), calls=%async_computation | async-start | bytes 1572864 | tf_op jit(solution)/shard_map/all_to_all | solution.py:71
  303.0 20.2 %all-to-all-done = bf16[4,2,49152]{2,1,0:T(2,128)(2,1)S(1)} async-done(((bf16[4,2,49152]{2,1,0:T(2,128)(2,1)}), bf16[4,2,49152]{2,1,0:T(2,128)(2,1)S(1)}, u32[]{:S(2)}, u32[]{:S(2)}) %all-to-all-start) | async-done | bytes 786464 | tf_op jit(solution)/shard_map/all_to_all | solution.py:71
  323.2 0.7 reshape.118
  324.2 1.0 copy.28
  325.2 2.7 dynamic-slice_bitcast_fusion
  327.9 7.8 %fusion.7 = (bf16[1,1024,768]{1,0,2:T(2,128)(2,1)S(1)}, bf16[1,1024,768]{1,0,2:T(2,128)(2,1)S(1)}) fusion(bf16[2,1024,768]{1,0,2:T(2,128)(2,1)} %all-gather.8.cloned.1.call-done), kind=kLoop, calls=%fused_computation.47 | loop fusion | bytes 6291456 | tf_op jit(solution)/shard_map/slice | solution.py:58
  335.7 0.6 copy.26
  336.3 0.6 copy.27
  336.9 1.9 select_select_fusion
  339.3 7.6 %convolution_convert_fusion = bf16[1024,512]{1,0:T(8,128)(2,1)} fusion(bf16[1024,6144]{0,1:T(8,128)(2,1)S(1)} %bitcast.33, bf16[6144,512]{1,0:T(8,128)(2,1)S(1)} %bitcast.45), kind=kOutput, calls=%fused_computation.10 | convolution fusion | flops 6442975232 | bytes 19922944 | tf_op jit(solution)/shard_map/dot_general | solution.py:60
  (28 shorter events, 1.9 us)
Async XLA Ops:
  7.2 3.8 %copy-start = (f32[8,96,512]{2,1,0:T(8,128)S(1)}, f32[8,96,512]{2,1,0:T(8,128)}, u32[]{:S(2)}) copy-start(f32[8,96,512]{2,1,0:T(8,128)} %param.11) | copy-start | bytes 4718596
  7.2 182.7 %all-gather.4.cloned.1.call-start = ((), (), s32[]{:S(2)}) async-start(), calls=%async_computation.1 | async-start | bytes 14155776 | tf_op jit(solution)/shard_map/all_gather | solution.py:20
  9.6 2.4 copy-start.2
  9.6 2.5 copy-start.1
  10.9 278.7 %all-gather.6.cloned.1.call-start = ((), (), s32[]{:S(2)}) async-start(), calls=%async_computation.2 | async-start | bytes 7077888 | tf_op jit(solution)/shard_map/all_gather | solution.py:21
  11.9 315.9 %all-gather.8.cloned.1.call-start = ((), (), s32[]{:S(2)}) async-start(), calls=%async_computation.3 | async-start | bytes 3932160 | tf_op jit(solution)/shard_map/all_gather | solution.py:48
  299.3 23.9 %all-to-all-start = ((bf16[4,2,49152]{2,1,0:T(2,128)(2,1)}), bf16[4,2,49152]{2,1,0:T(2,128)(2,1)S(1)}, u32[]{:S(2)}, u32[]{:S(2)}) async-start(bf16[4,2,49152]{2,1,0:T(2,128)(2,1)} %reshape.117), calls=%async_computation | async-start | bytes 1572864 | tf_op jit(solution)/shard_map/all_to_all | solution.py:71
  336.3 2.5 slice-start
  336.9 2.4 slice-start.1
Sparse Core Ops, SparseCore 0:
  11.0 178.8 all-gather.3
  192.6 96.8 all-gather.5
  291.7 35.1 all-gather.7

commit v2 on v1

--- a/solution.py
+++ b/solution.py
@@ -1,12 +1,16 @@
+import functools
+
 import jax
 import jax.numpy as jnp
 from jax import lax
+from jax.experimental import pallas as pl
+from jax.experimental.pallas import tpu as pltpu
 from jax.sharding import PartitionSpec as P
 
 epsilon = 1e-06
 
 
-def on_device(tokens, norm_gain, gate_train, up_train, down_train, expert_ids, route_weights):
+def gathered(tokens, norm_gain, gate_train, up_train, down_train, expert_ids, route_weights):
     experts, rows, cols = gate_train.shape
     fs_at = lax.axis_index("fs")
     tok_rows, picks = expert_ids.shape
@@ -72,6 +76,339 @@
     return own[None, :, :cols], own[None, :, cols:], down_serve, mixed
 
 
+def ring_kernel(
+    n, tp_count, blocks, gu_ref, dn_ref, normed_ref, ids_ref, shares_ref,
+    main_ref, tail_ref, serve_ref, mixed_ref,
+    gu_all, dn_all, picked, picked_all, total,
+    send_sem, recv_sem, pick_send, pick_recv, serve_send, serve_recv, serve_copy, own_sem,
+):
+    fs_at, tp_at = lax.axis_index("fs"), lax.axis_index("tp")
+    experts, down_rows, down_cols = dn_ref.shape
+    rows = gu_ref.shape[1]
+    tok_rows = normed_ref.shape[0]
+    half = experts // 2
+    last = n // 2
+
+    place = (1 - fs_at % 2) * (fs_at // 2) + (fs_at % 2) * (n - 1 - fs_at // 2)
+
+    def index_at(step):
+        at = (place + step + n) % n
+        odd = at // last
+        return (1 - odd) * (2 * at) + odd * (2 * (n - 1 - at) + 1)
+
+    right, left = index_at(1), index_at(-1)
+    barrier = pltpu.get_barrier_semaphore()
+    for to in (right, left):
+        pl.semaphore_signal(
+            barrier, inc=1, device_id={"fs": to}, device_id_type=pl.DeviceIdType.MESH
+        )
+    for hop in range(1, tp_count):
+        pl.semaphore_signal(
+            barrier, inc=1, device_id={"tp": (tp_at + hop) % tp_count},
+            device_id_type=pl.DeviceIdType.MESH,
+        )
+    pl.semaphore_wait(barrier, 1 + tp_count)
+
+    def landing(unit, source):
+        if unit < 2:
+            return gu_all.at[unit, pl.ds(pl.multiple_of(source * rows, rows), rows), :]
+        return dn_all.at[
+            source // 2, pl.ds((unit - 2) * half, half),
+            pl.ds(pl.multiple_of((source % 2) * down_rows, down_rows), down_rows), :,
+        ]
+
+    def message(way, step, unit):
+        source = index_at(1 - step if way == 0 else step - 1)
+        place_of = landing(unit, source)
+        if step == 1:
+            src = gu_ref.at[unit] if unit < 2 else dn_ref.at[pl.ds((unit - 2) * half, half)]
+        else:
+            src = place_of
+        return pltpu.make_async_remote_copy(
+            src_ref=src, dst_ref=place_of,
+            send_sem=send_sem.at[way, step - 1, unit], recv_sem=recv_sem.at[way, step - 1, unit],
+            device_id={"fs": right if way == 0 else left},
+            device_id_type=pl.DeviceIdType.MESH,
+        )
+
+    started = []
+
+    def send(way, step, unit):
+        if step < last or (step == last and unit % 2 == way):
+            message(way, step, unit).start()
+            started.append((way, step, unit))
+
+    def receive(way, step, unit):
+        if step < last or (step == last and unit % 2 == way):
+            source = index_at(-step if way == 0 else step)
+            place_of = landing(unit, source)
+            pltpu.make_async_remote_copy(
+                src_ref=place_of, dst_ref=place_of,
+                send_sem=send_sem.at[way, step - 1, unit],
+                recv_sem=recv_sem.at[way, step - 1, unit],
+                device_id={"fs": right if way == 0 else left},
+                device_id_type=pl.DeviceIdType.MESH,
+            ).wait_recv()
+
+    def relay(step, unit):
+        for way in (0, 1):
+            receive(way, step, unit)
+            if step < last:
+                send(way, step + 1, unit)
+
+    for unit in (0, 1):
+        for way in (0, 1):
+            send(way, 1, unit)
+    own = [
+        pltpu.make_async_copy(gu_ref.at[unit], landing(unit, fs_at), own_sem.at[unit])
+        for unit in (0, 1)
+    ] + [
+        pltpu.make_async_copy(
+            dn_ref.at[pl.ds((unit - 2) * half, half)], landing(unit, fs_at), own_sem.at[unit]
+        )
+        for unit in (2, 3)
+    ]
+    for copy in own:
+        copy.start()
+
+    serves = []
+
+    def serve(step):
+        source = index_at(step)
+        to = source // 2
+        src = dn_all.at[
+            source // 2, fs_at,
+            pl.ds(pl.multiple_of((source % 2) * down_rows, down_rows), down_rows), :,
+        ]
+        dst = serve_ref.at[
+            pl.ds(pl.multiple_of((source % 2) * down_rows, down_rows), down_rows),
+            pl.ds(pl.multiple_of(tp_at * down_cols, down_cols), down_cols),
+        ]
+        slot = len(serves)
+        remote = pltpu.make_async_remote_copy(
+            src_ref=src, dst_ref=dst, send_sem=serve_send.at[slot],
+            recv_sem=serve_recv.at[source % 2, tp_at],
+            device_id={"tp": to}, device_id_type=pl.DeviceIdType.MESH,
+        )
+        local = pltpu.make_async_copy(src, dst, serve_copy.at[slot])
+        pl.when(to != tp_at)(remote.start)
+        pl.when(to == tp_at)(local.start)
+        serves.append((to, remote, local))
+
+    for step in range(1, last):
+        for unit in (0, 1):
+            relay(step, unit)
+    for unit in (2, 3):
+        for way in (0, 1):
+            send(way, 1, unit)
+    for copy in own:
+        copy.wait()
+    serve(0)
+    for unit in (0, 1):
+        relay(last, unit)
+
+    lane = lax.broadcasted_iota(jnp.int32, (1, 384), 1)
+    parity = jnp.where(lane < 256, lane // 128, (lane - 256) // 64)
+    low = lax.broadcasted_iota(jnp.int32, (1, 128), 1) < 64
+    height = tok_rows // blocks
+    picks = []
+
+    def evaluate(block):
+        at = block * height
+        tokens = normed_ref[pl.ds(at, height), :]
+        ids = [ids_ref[pl.ds(at, height), pl.ds(k, 1)] for k in (0, 1)]
+        folded = [jnp.zeros((height, 384), jnp.float32) for _ in (0, 1)]
+        for first in range(0, half, 2):
+            span = pl.ds(first * 384, 768)
+            gate = jnp.dot(tokens, gu_all[0, :, span], preferred_element_type=jnp.float32)
+            up = jnp.dot(tokens, gu_all[1, :, span], preferred_element_type=jnp.float32)
+            hidden = gate / (1.0 + jnp.exp(-gate)) * up
+            for pair in (0, 1):
+                part = hidden[:, pair * 384 : (pair + 1) * 384]
+                named = 2 * (first + pair) + parity
+                for k in (0, 1):
+                    folded[k] = folded[k] + jnp.where(ids[k] == named, part, 0.0)
+        folded = [folded[k] * shares_ref[pl.ds(at, height), pl.ds(k, 1)] for k in (0, 1)]
+        ends = [f[:, 256:384] + pltpu.roll(f[:, 256:384], 64, 1) for f in folded]
+        for k in (0, 1):
+            main = folded[k][:, :128] + folded[k][:, 128:256]
+            picked[pl.ds(at, height), pl.ds(k * 128, 128)] = main.astype(jnp.bfloat16)
+        picked[pl.ds(at, height), pl.ds(256, 128)] = jnp.where(low, ends[0], ends[1]).astype(
+            jnp.bfloat16
+        )
+        for hop in range(1, tp_count):
+            copy = pltpu.make_async_remote_copy(
+                src_ref=picked.at[pl.ds(at, height), :],
+                dst_ref=picked_all.at[tp_at, pl.ds(at, height), :],
+                send_sem=pick_send.at[hop - 1, block], recv_sem=pick_recv.at[hop - 1, block],
+                device_id={"tp": (tp_at + hop) % tp_count},
+                device_id_type=pl.DeviceIdType.MESH,
+            )
+            copy.start()
+            picks.append(copy)
+        picked_all[tp_at, pl.ds(at, height), :] = picked[pl.ds(at, height), :]
+
+    events = [(step, unit) for step in range(1, last) for unit in (2, 3)]
+
+    def event():
+        step, unit = events.pop(0)
+        relay(step, unit)
+        if unit == 3:
+            serve(-step)
+            serve(step)
+
+    for block in range(blocks):
+        evaluate(block)
+        if block > 0:
+            event()
+
+    main_at = pl.multiple_of((fs_at // 2) * 384 + (fs_at % 2) * 128, 128)
+    tail_at = pl.multiple_of((fs_at // 2) * 384 + 256, 128)
+    main_ref[...] = gu_all[:, :, pl.ds(main_at, 128)]
+    tail_ref[...] = gu_all[:, :, pl.ds(tail_at, 128)]
+
+    while events:
+        event()
+    for hop in range(1, tp_count):
+        for block in range(blocks):
+            picks[block * (tp_count - 1) + hop - 1].wait()
+
+    def project(index, first):
+        for block in range(blocks):
+            at = block * height
+            ids = [ids_ref[pl.ds(at, height), pl.ds(k, 1)] for k in (0, 1)]
+            held = picked_all[index, pl.ds(at, height), :].astype(jnp.float32)
+            end = held[:, 256:384]
+            turned = pltpu.roll(end, 64, 1)
+            ends = [jnp.where(low, end, turned), jnp.where(low, turned, end)]
+            pieces, weights = [], []
+            for pair in range(half):
+                for e in (2 * pair, 2 * pair + 1):
+                    pieces.append(
+                        jnp.where(ids[0] == e, held[:, :128],
+                                  jnp.where(ids[1] == e, held[:, 128:256], 0.0))
+                    )
+                    weights.append(dn_all[index, e, pl.ds(0, 128), :])
+                named = 2 * pair + parity[:, 256:384]
+                pieces.append(
+                    jnp.where(ids[0] == named, ends[0], jnp.where(ids[1] == named, ends[1], 0.0))
+                )
+                for e in (2 * pair, 2 * pair + 1):
+                    weights.append(dn_all[index, e, pl.ds(128, 64), :])
+            spread = jnp.concatenate([p.astype(jnp.bfloat16) for p in pieces], axis=1)
+            product = jnp.dot(
+                spread, jnp.concatenate(weights, axis=0), preferred_element_type=jnp.float32
+            )
+            if first:
+                total[pl.ds(at, height), :] = product
+            else:
+                total[pl.ds(at, height), :] += product
+
+    far = index_at(last) // 2
+    project((far + 1) % last, True)
+
+    def middle(step, carry):
+        project((far + step) % last, False)
+        return carry
+
+    lax.fori_loop(2, last, middle, 0)
+    for unit in (2, 3):
+        relay(last, unit)
+    serve(last)
+    project(far, False)
+    mixed_ref[...] = total[...].astype(jnp.bfloat16)
+
+    for way, step, unit in started:
+        message(way, step, unit).wait_send()
+    for to, remote, local in serves:
+        pl.when(to != tp_at)(remote.wait_send)
+        pl.when(to == tp_at)(local.wait)
+    for part in (0, 1):
+        for source in range(tp_count):
+            dst = serve_ref.at[
+                pl.ds(part * down_rows, down_rows), pl.ds(source * down_cols, down_cols)
+            ]
+            arrival = pltpu.make_async_remote_copy(
+                src_ref=dst, dst_ref=dst, send_sem=serve_send.at[0],
+                recv_sem=serve_recv.at[part, source],
+                device_id={"tp": (tp_at + 1) % tp_count}, device_id_type=pl.DeviceIdType.MESH,
+            )
+            pl.when(tp_at != source)(arrival.wait_recv)
+
+
+def ringed(tokens, norm_gain, gate_train, up_train, down_train, expert_ids, route_weights):
+    experts, rows, cols = gate_train.shape
+    down_rows, down_cols = down_train.shape[1:]
+    n, tp_count = lax.axis_size("fs"), lax.axis_size("tp")
+    tok_rows, width = tokens.shape
+    half = experts // 2
+    blocks = 4
+
+    def paired(train):
+        value = (norm_gain[None, :, None] * train).astype(jnp.bfloat16)
+        value = value.transpose(1, 0, 2).reshape(rows, half, 2, cols)
+        return jnp.concatenate(
+            [value[..., :128].reshape(rows, half, 256), value[..., 128:].reshape(rows, half, 128)],
+            axis=2,
+        ).reshape(rows, half * 384)
+
+    tok_float = tokens.astype(jnp.float32)
+    normed = (
+        tok_float * lax.rsqrt(jnp.mean(tok_float * tok_float, axis=-1, keepdims=True) + epsilon)
+    ).astype(jnp.bfloat16)
+    shares = route_weights / jnp.sum(route_weights, axis=-1, keepdims=True)
+    vmem = pl.BlockSpec(memory_space=pltpu.VMEM)
+    dma = pltpu.SemaphoreType.DMA
+    main, tail, serve, mixed = pl.pallas_call(
+        functools.partial(ring_kernel, n, tp_count, blocks),
+        out_shape=(
+            jax.ShapeDtypeStruct((2, width, 128), jnp.bfloat16),
+            jax.ShapeDtypeStruct((2, width, 128), jnp.bfloat16),
+            jax.ShapeDtypeStruct((2 * down_rows, width), jnp.bfloat16),
+            jax.ShapeDtypeStruct((tok_rows, down_cols), jnp.bfloat16),
+        ),
+        in_specs=[vmem] * 5,
+        out_specs=(vmem,) * 4,
+        scratch_shapes=[
+            pltpu.VMEM((2, width, half * 384), jnp.bfloat16),
+            pltpu.VMEM((n // 2, experts, 2 * down_rows, down_cols), jnp.bfloat16),
+            pltpu.VMEM((tok_rows, 384), jnp.bfloat16),
+            pltpu.VMEM((tp_count, tok_rows, 384), jnp.bfloat16),
+            pltpu.VMEM((tok_rows, down_cols), jnp.float32),
+            dma((2, n // 2, 4)),
+            dma((2, n // 2, 4)),
+            dma((tp_count - 1, blocks)),
+            dma((tp_count - 1, blocks)),
+            dma((n,)),
+            dma((2, tp_count)),
+            dma((n,)),
+            dma((4,)),
+        ],
+        compiler_params=pltpu.CompilerParams(
+            collective_id=0, has_side_effects=True, vmem_limit_bytes=60 * 1024 * 1024
+        ),
+    )(
+        jnp.stack([paired(gate_train), paired(up_train)]), down_train.astype(jnp.bfloat16),
+        normed, expert_ids, shares,
+    )
+    odd = lax.axis_index("fs") % 2
+    whole = jnp.concatenate(
+        [main, jnp.where(odd == 1, tail[..., 64:], tail[..., :64])], axis=2
+    )
+    return whole[0:1], whole[1:2], serve[None], mixed
+
+
+def on_device(tokens, norm_gain, gate_train, up_train, down_train, expert_ids, route_weights):
+    experts, rows, cols = gate_train.shape
+    n, tp_count = lax.axis_size("fs"), lax.axis_size("tp")
+    fits = experts == n and n == 2 * tp_count and cols == 192 and expert_ids.shape[1] == 2
+    held = 3 * experts * n * rows * cols * 2
+    run = ringed if fits and held < 24 * 1024 * 1024 else gathered
+    return run(
+        tokens, norm_gain, gate_train, up_train, down_train, expert_ids, route_weights
+    )
+
+
 def solution(mesh):
     return jax.shard_map(
         on_device,

time: 354 us -> 218 us (0.62)
  waiting for transfers between devices: 266 us -> 0 us
  Pallas kernels: 0 us -> 195 us
  matrix products: 24.7 us -> 0 us
  local copies, waits for them, and re-layouts: 20.5 us -> 7.23 us
  between operations: 14 us -> 0.84 us
  other arithmetic: 24.4 us -> 14.2 us
  starting transfers between devices: 3.8 us -> 0 us
    all_gather x3 -> x0, waiting for transfers between devices: 246 us -> none  [the longest x1 175 us: on_device(): gate_up_all = lax.all_gather(gate_up, 'fs', axis=0, tiled=True)]
    pallas_call x0 -> x1, Pallas kernels: none -> 195 us  [ringed(): pl.pallas_call(functools.partial(ring_kernel, n, tp_count, blocks), out_s...]
    dot_general x2 -> x0, matrix products: 24.7 us -> none  [the longest x1 17.1 us: on_device(): acts = jnp.dot(normed, part, preferred_element_type=jnp.float32)]
    all_to_all x1 -> x0, waiting for transfers between devices: 20.2 us -> none  [on_device(): lax.all_to_all(down_own, 'tp', split_axis=1, concat_axis=2, tiled=True)]
    another operation x4 -> x1, other arithmetic: 11.5 us -> 1.33 us  [ringed(): jnp.stack([paired(gate_train), paired(up_train)])]
    slice x3 -> x4, local copies, waits for them, and re-layouts: 7.83 us -> 0.11 us  [the longest x2 0.07 us: paired(): value[..., :128].reshape(rows, half, 256)]
    convert_element_type x1 -> x3, other arithmetic: 0.98 us -> 7.78 us  [the longest x1 2.88 us: ringed(): down_train.astype(jnp.bfloat16)]
    unnamed x2 -> x0, other arithmetic: 5.43 us -> none
  transfers between devices with their start and end apart: 4 -> 0, of which waited for: 3 -> 0; matrix products, arithmetic and copies ran while one was open for 13% -> 0% of each run, Pallas kernels for 0% -> 0%
where the time goes in v2:
time: 218 us; the launch traced here: 217 us
  Pallas kernels  195 us (89%)
  other arithmetic  14.2 us (7%)
  local copies, waits for them, and re-layouts  7.23 us (3%)
    pallas_call x1, Pallas kernels, ringed(): pl.pallas_call(functools.partial(ring_kernel, n, tp_count, blocks), out_s...  195 us
    unnamed x18, local copies, waits for them, and re-layouts  5.59 us

profile of v2, /device:TPU:0, one launch (start us, length us, event | category | flops | bytes accessed | tf_op | source)
XLA Modules:
  0.0 217.4 jit_solution(3769784616216098644)
XLA Ops:
  0.6 2.2 %multiply_convert_fusion.1 = (bf16[8,256,192]{1,2,0:T(8,128)(2,1)S(1)}, bf16[8,256,192]{1,2,0:T(8,128)(2,1)S(1)}) fusion(f32[8,256,192]{1,2,0:T(8,128)} %param.9, f32[256]{0:T(256)} %param.8, f32[8,256,192]{1,2,0:T(8,128)} %param.10), kind=kLoop, calls=%fused_computation.8 | loop fusion | flops 1572864 | bytes 4719616 | tf_op jit(solution)/shard_map/convert_element_type | solution.py:348
  2.9 0.2 copy.30
  3.1 0.3 copy.29
  3.4 0.4 pad_maximum_fusion.3
  3.8 0.3 stack_reshape.7
  4.1 0.2 copy.28
  4.4 0.3 copy.27
  4.7 0.4 pad_maximum_fusion.2
  5.1 0.3 stack_reshape.6
  5.4 0.0 copy-start
  5.4 1.3 pad_maximum_fusion.gu_ref
  6.7 2.9 %convert_element_type.17.dn_ref = bf16[8,96,512]{2,1,0:T(8,128)(2,1)} convert(f32[8,96,512]{2,1,0:T(8,128)} %param.11) | non-fusion elementwise | flops 393216 | bytes 2359296 | tf_op jit(solution)/shard_map/convert_element_type | solution.py:391
  9.6 0.9 fusion
  10.5 2.7 %fusion.1.normed_ref = bf16[1024,2048]{1,0:T(8,128)(2,1)} fusion(bf16[1024,2048]{1,0:T(8,128)(2,1)S(1)} %copy-done, f32[1024]{0:T(1024)S(1)} %add_rsqrt_fusion), kind=kLoop, calls=%fused_computation.3 | loop fusion | flops 6291456 | bytes 8392704 | tf_op jit(solution)/shard_map/convert_element_type | solution.py:358
  13.2 1.0 copy.33.ids_ref
  14.2 0.2 copy.31
  14.5 1.0 broadcast_divide_fusion.shares_ref
  15.5 195.2 %shard_map.102 = (bf16[2,2048,128]{2,1,0:T(8,128)(2,1)}, bf16[2,2048,128]{2,1,0:T(8,128)(2,1)}, bf16[192,2048]{1,0:T(8,128)(2,1)}, bf16[1024,512]{1,0:T(8,128)(2,1)}) custom-call(bf16[2,256,1536]{2,1,0:T(8,128)(2,1)} %pad_maximum_fusion.gu_ref, bf16[8,96,512]{2,1,0:T(8,128)(2,1)} %convert_element_type.17.dn_ref, bf16[1024,2048]{1,0:T(8,128)(2,1)} %fusion.1.normed_ref, ...), custom_call_target="tpu_custom_call" | custom-call | tf_op jit(solution)/shard_map/pallas_call | solution.py:362
  210.7 2.0 slice_select_fusion
  212.7 0.4 pad_maximum_fusion.1
  213.1 1.2 copy.34
  214.4 1.2 copy.35
  215.6 0.9 copy.38
  216.5 1.0 copy.39
  (17 shorter events, 0.2 us)
Async XLA Ops:
  5.4 4.2 %copy-start = (bf16[1024,2048]{1,0:T(8,128)(2,1)S(1)}, bf16[1024,2048]{1,0:T(8,128)(2,1)}, u32[]{:S(2)}) copy-start(bf16[1024,2048]{1,0:T(8,128)(2,1)} %param.7) | copy-start | bytes 12582916
  10.5 2.7 %copy-start.5 = (s32[1024,2]{0,1:T(2,128)S(1)}, s32[1024,2]{0,1:T(2,128)}, u32[]{:S(2)}) copy-start(s32[1024,2]{0,1:T(2,128)} %param.12) | copy-start | bytes 24580
  10.5 3.7 %copy-start.4 = (f32[1024,2]{0,1:T(2,128)S(1)}, f32[1024,2]{0,1:T(2,128)}, u32[]{:S(2)}) copy-start(f32[1024,2]{0,1:T(2,128)} %param.13) | copy-start | bytes 24580
  210.7 2.0 copy-start.2
  213.1 2.5 %copy-start.3 = (bf16[192,2048]{1,0:T(8,128)(2,1)S(1)}, bf16[192,2048]{1,0:T(8,128)(2,1)}, u32[]{:S(2)}) copy-start(bf16[192,2048]{1,0:T(8,128)(2,1)} %get-tuple-element.10) | copy-start | bytes 2359300
  214.4 2.1 copy-start.1

commit v3 on v2

--- a/solution.py
+++ b/solution.py
@@ -77,7 +77,7 @@
 
 
 def ring_kernel(
-    n, tp_count, blocks, gu_ref, dn_ref, normed_ref, ids_ref, shares_ref,
+    n, tp_count, blocks, gu_ref, dn_ref, tokens_ref, ids_ref, routes_ref,
     main_ref, tail_ref, serve_ref, mixed_ref,
     gu_all, dn_all, picked, picked_all, total,
     send_sem, recv_sem, pick_send, pick_recv, serve_send, serve_recv, serve_copy, own_sem,
@@ -85,7 +85,7 @@
     fs_at, tp_at = lax.axis_index("fs"), lax.axis_index("tp")
     experts, down_rows, down_cols = dn_ref.shape
     rows = gu_ref.shape[1]
-    tok_rows = normed_ref.shape[0]
+    tok_rows = tokens_ref.shape[0]
     half = experts // 2
     last = n // 2
 
@@ -215,7 +215,9 @@
 
     def evaluate(block):
         at = block * height
-        tokens = normed_ref[pl.ds(at, height), :]
+        tokens = tokens_ref[pl.ds(at, height), :].astype(jnp.float32)
+        square = jnp.mean(tokens * tokens, axis=-1, keepdims=True)
+        tokens = (tokens * lax.rsqrt(square + epsilon)).astype(jnp.bfloat16)
         ids = [ids_ref[pl.ds(at, height), pl.ds(k, 1)] for k in (0, 1)]
         folded = [jnp.zeros((height, 384), jnp.float32) for _ in (0, 1)]
         for first in range(0, half, 2):
@@ -228,7 +230,8 @@
                 named = 2 * (first + pair) + parity
                 for k in (0, 1):
                     folded[k] = folded[k] + jnp.where(ids[k] == named, part, 0.0)
-        folded = [folded[k] * shares_ref[pl.ds(at, height), pl.ds(k, 1)] for k in (0, 1)]
+        routes = [routes_ref[pl.ds(at, height), pl.ds(k, 1)] for k in (0, 1)]
+        folded = [folded[k] * (routes[k] / (routes[0] + routes[1])) for k in (0, 1)]
         ends = [f[:, 256:384] + pltpu.roll(f[:, 256:384], 64, 1) for f in folded]
         for k in (0, 1):
             main = folded[k][:, :128] + folded[k][:, 128:256]
@@ -352,11 +355,6 @@
             axis=2,
         ).reshape(rows, half * 384)
 
-    tok_float = tokens.astype(jnp.float32)
-    normed = (
-        tok_float * lax.rsqrt(jnp.mean(tok_float * tok_float, axis=-1, keepdims=True) + epsilon)
-    ).astype(jnp.bfloat16)
-    shares = route_weights / jnp.sum(route_weights, axis=-1, keepdims=True)
     vmem = pl.BlockSpec(memory_space=pltpu.VMEM)
     dma = pltpu.SemaphoreType.DMA
     main, tail, serve, mixed = pl.pallas_call(
@@ -389,7 +387,7 @@
         ),
     )(
         jnp.stack([paired(gate_train), paired(up_train)]), down_train.astype(jnp.bfloat16),
-        normed, expert_ids, shares,
+        tokens, expert_ids, route_weights,
     )
     odd = lax.axis_index("fs") % 2
     whole = jnp.concatenate(

time: 218 us -> 213 us (0.977)
  other arithmetic: 14.2 us -> 7.66 us
    convert_element_type x1 -> x0, other arithmetic: 2.69 us -> none  [ringed(): normed = (tok_float * lax.rsqrt(jnp.mean(tok_float * tok_float, axis=-1,...]
where the time goes in v3:
time: 213 us
  Pallas kernels  195 us (92%)
  local copies, waits for them, and re-layouts  8.71 us (4%)
  other arithmetic  7.66 us (4%)
    pallas_call x1, Pallas kernels, ringed(): pl.pallas_call(functools.partial(ring_kernel, n, tp_count, blocks), out_s...  195 us
    unnamed x18, local copies, waits for them, and re-layouts  7.06 us

profile of v3, /device:TPU:0, one launch (start us, length us, event | category | flops | bytes accessed | tf_op | source)
XLA Modules:
  0.0 212.6 jit_solution(9932086685451836143)
XLA Ops:
  0.6 2.2 %multiply_convert_fusion.1 = (bf16[8,256,192]{1,2,0:T(8,128)(2,1)S(1)}, bf16[8,256,192]{1,2,0:T(8,128)(2,1)S(1)}) fusion(f32[8,256,192]{1,2,0:T(8,128)} %param.9, f32[256]{0:T(256)} %param.8, f32[8,256,192]{1,2,0:T(8,128)} %param.10), kind=kLoop, calls=%fused_computation.4 | loop fusion | flops 1572864 | bytes 4719616 | tf_op jit(solution)/shard_map/convert_element_type | solution.py:351
  2.9 0.2 copy.22
  3.1 0.3 copy.21
  3.4 0.4 pad_maximum_fusion.3
  3.8 0.3 stack_reshape.7
  4.1 0.2 copy.20
  4.4 0.3 copy.19
  4.7 0.4 pad_maximum_fusion.2
  5.1 0.3 stack_reshape.6
  5.4 0.0 copy-start
  5.4 1.3 pad_maximum_fusion.gu_ref
  6.7 0.7 copy-done
  7.4 1.0 convert_element_type.11.dn_ref
  8.3 0.0 copy-done.4
  8.4 1.0 copy.23.ids_ref
  9.4 1.0 copy.24.routes_ref
  10.4 195.5 %shard_map.102 = (bf16[2,2048,128]{2,1,0:T(8,128)(2,1)}, bf16[2,2048,128]{2,1,0:T(8,128)(2,1)}, bf16[192,2048]{1,0:T(8,128)(2,1)}, bf16[1024,512]{1,0:T(8,128)(2,1)}) custom-call(bf16[2,256,1536]{2,1,0:T(8,128)(2,1)} %pad_maximum_fusion.gu_ref, bf16[8,96,512]{2,1,0:T(8,128)(2,1)} %convert_element_type.11.dn_ref, bf16[1024,2048]{1,0:T(8,128)(2,1)} %tokens_ref.1, ...), custom_call_target="tpu_custom_call" | custom-call | tf_op jit(solution)/shard_map/pallas_call | solution.py:360
  205.9 2.0 slice_select_fusion
  207.9 0.0 copy-done.2
  207.9 0.4 pad_maximum_fusion.1
  208.3 1.2 copy.25
  209.6 1.2 copy.26
  210.8 0.9 copy.29
  211.7 1.0 copy.30
  (12 shorter events, 0.1 us)
Async XLA Ops:
  5.4 2.0 copy-start
  7.4 1.0 copy-start.4
  7.4 2.0 copy-start.5
  205.9 2.0 copy-start.2
  208.3 2.5 %copy-start.3 = (bf16[192,2048]{1,0:T(8,128)(2,1)S(1)}, bf16[192,2048]{1,0:T(8,128)(2,1)}, u32[]{:S(2)}) copy-start(bf16[192,2048]{1,0:T(8,128)(2,1)} %get-tuple-element.10) | copy-start | bytes 2359300
  209.5 2.1 copy-start.1
